TPU v7x, 32 devices: a whole 2x2x4 slice. The times are simulated.
32 devices in a mesh: grp: 2 (over y), sp: 4 (over z), tp: 4 (over x, core).
Axes of the slice: x: 2, y: 2, z: 4, core: 2. Of those that a mesh axis runs over, the one named last changes fastest.
Arguments:
- resid_in: bfloat16 [2048, 2048], P(('grp', 'sp', 'tp')), parts along dimension 0, may hold values from -3 to 3
- queries: bfloat16 [2048, 1024], P(('grp', 'sp'), 'tp'), parts along dimension 0, may hold values from -39 to 39
- keys: bfloat16 [2048, 1024], P(('grp', 'sp'), 'tp'), parts along dimension 0, may hold values from -6 to 6
- values: bfloat16 [2048, 1024], P(('grp', 'sp'), 'tp'), parts along dimension 0, may hold values from -12 to 12
- cum_gate: float32 [2048, 16], P('grp', 'tp'), parts along dimension 0, may hold values from -105 to 0, as said below
- w_out: bfloat16 [1024, 2048], replicated, may hold values from -0.1875 to 0.1875
- norm_gain: float32 [2048], replicated, may hold values from 0.1 to 1.9
- w_gate: bfloat16 [2048, 5632], P('sp', 'tp'), may hold values from -0.125 to 0.125
- w_up: bfloat16 [2048, 5632], P('sp', 'tp'), may hold values from -0.125 to 0.125
- w_down: bfloat16 [5632, 2048], P('tp', 'sp'), may hold values from -0.078125 to 0.078125
Outputs:
- resid_out: bfloat16 [2048, 2048], P(('grp', 'sp', 'tp')), parts along dimension 0
There are 2 independent parts, one for each index of `grp`. A program takes and returns all parts, laid end to end along the dimension named above; an argument that names none is the same for every part. Nothing has to cross between parts.
Inputs may be any that keep to these rules, and one draw needn't show every extreme that they name: `cum_gate`: in every head the values never rise from one position to the next, and the first is at most 0.
All inputs are finite; a program needn't handle non-finite values.
Results may differ from a plain program's by a relative error of at most 0.018.
Values may be sent and summed in bfloat16 or wider, within the bound.
A program may use at most 128 MiB of HBM per device.

v0:
```python
import math
import jax
import jax.numpy as jnp
from jax import lax
from jax.sharding import PartitionSpec as P

HEAD_DIM = 64


def on_device(resid_in, queries, keys, values, cum_gate, w_out, norm_gain, w_gate, w_up, w_down):
    tok_rows = queries.shape[0]
    local_heads = queries.shape[1] // HEAD_DIM
    scale = HEAD_DIM ** (-0.5)
    offset = lax.axis_index("sp") * tok_rows
    query_heads = queries.reshape(tok_rows, local_heads, HEAD_DIM)
    own_gate = lax.dynamic_slice_in_dim(cum_gate, offset, tok_rows, 0).T
    query_pos = offset + jnp.arange(tok_rows, dtype=jnp.int32)
    last_pos = offset + tok_rows - 1
    initial = (
        jnp.full((local_heads, tok_rows), -1e30, jnp.float32),
        jnp.zeros((local_heads, tok_rows), jnp.float32),
        jnp.zeros((tok_rows, local_heads, HEAD_DIM), jnp.float32),
    )
    key_piece = lax.all_gather(keys, "sp", axis=0, tiled=True)
    value_piece = lax.all_gather(values, "sp", axis=0, tiled=True)
    length = key_piece.shape[0]
    span = math.gcd(length, 512)

    def block(index, state):
        begin = index * span

        def work(inner):
            maxima, totals, summed = inner
            key_block = lax.dynamic_slice_in_dim(key_piece, index * span, span, 0).reshape(
                span, local_heads, HEAD_DIM
            )
            value_block_rows = lax.dynamic_slice_in_dim(value_piece, index * span, span, 0).reshape(
                span, local_heads, HEAD_DIM
            )
            key_gate = lax.dynamic_slice_in_dim(cum_gate, begin, span, 0).T
            scores = (
                jnp.einsum(
                    "qhd,khd->hqk", query_heads, key_block, preferred_element_type=jnp.float32
                )
                * scale
            )
            scores = scores + own_gate[:, :, None] - key_gate[:, None, :]
            key_pos = begin + jnp.arange(span, dtype=jnp.int32)
            mask = (key_pos[None, :] <= query_pos[:, None])[None]
            scores = jnp.where(mask, scores, -1e30)
            new_max = jnp.maximum(maxima, jnp.max(scores, axis=-1))
            weights = jnp.where(mask, jnp.exp(scores - new_max[:, :, None]), 0.0)
            rescale = jnp.exp(maxima - new_max)
            totals = totals * rescale + jnp.sum(weights, axis=-1)
            product = jnp.einsum(
                "hqk,khd->qhd",
                weights.astype(jnp.bfloat16),
                value_block_rows,
                preferred_element_type=jnp.float32,
            )
            summed = summed * rescale.T[:, :, None] + product
            return (new_max, totals, summed)

        return lax.cond(begin <= last_pos, work, lambda inner: inner, state)

    maxima, totals, summed = lax.fori_loop(0, length // span, block, initial)
    attended = (
        (summed / totals.T[:, :, None])
        .reshape(tok_rows, local_heads * HEAD_DIM)
        .astype(jnp.bfloat16)
    )
    head_rows = lax.all_to_all(attended, "tp", split_axis=0, concat_axis=1, tiled=True)
    mixed = jnp.dot(head_rows, w_out, preferred_element_type=jnp.float32)
    resid = resid_in.astype(jnp.float32) + mixed
    normed = resid * lax.rsqrt(jnp.mean(resid * resid, axis=-1, keepdims=True) + 1e-06)
    normed = (normed * norm_gain).astype(jnp.bfloat16)
    all_rows = lax.all_gather(normed, "tp", axis=0, tiled=True)
    full_gate, full_up, full_down = (
        lax.all_gather(w_gate, "sp", axis=0, tiled=True),
        lax.all_gather(w_up, "sp", axis=0, tiled=True),
        lax.all_gather(w_down, "sp", axis=1, tiled=True),
    )
    gate = jnp.dot(all_rows, full_gate, preferred_element_type=jnp.float32)
    up = jnp.dot(all_rows, full_up, preferred_element_type=jnp.float32)
    hidden = (jax.nn.silu(gate) * up).astype(jnp.bfloat16)
    terms = jnp.dot(hidden, full_down, preferred_element_type=jnp.float32)
    back = lax.psum_scatter(
        terms.astype(jnp.bfloat16), "tp", scatter_dimension=0, tiled=True
    ).astype(jnp.float32)
    return (resid + back).astype(jnp.bfloat16)


def solution(mesh):
    return jax.shard_map(
        on_device,
        mesh=mesh,
        in_specs=(
            P(("grp", "sp", "tp"), None),
            P(("grp", "sp"), "tp"),
            P(("grp", "sp"), "tp"),
            P(("grp", "sp"), "tp"),
            P("grp", "tp"),
            P(),
            P(),
            P("sp", "tp"),
            P("sp", "tp"),
            P("tp", "sp"),
        ),
        out_specs=P(("grp", "sp", "tp"), None),
        check_vma=False,
    )
```

profile of v0, /device:TPU:0, one launch (start us, length us, event | category | flops | bytes accessed | tf_op | source)
XLA Modules:
  0.0 436.8 jit_solution(10608171273558845246)
XLA Ops:
  6.5 1.0 copy.16
  7.6 17.4 %all_gather.18 = bf16[1024,256]{0,1:T(8,128)(2,1)S(1)} all-gather(bf16[256,256]{0,1:T(8,128)(2,1)S(1)} %copy.16), channel_id=1, replica_groups=mesh['grp'=2,'sp'=4,'tp'=4] {'sp'}, dimensions={0}, use_global_device_ids=true | all-gather | bytes 655360 | tf_op jit(solution)/shard_map/all_gather | solution.py:24
  24.9 1.0 copy.18
  25.9 16.3 %all_gather.19 = bf16[1024,256]{0,1:T(8,128)(2,1)S(1)} all-gather(bf16[256,256]{0,1:T(8,128)(2,1)S(1)} %copy.18), channel_id=1, replica_groups=mesh['grp'=2,'sp'=4,'tp'=4] {'sp'}, dimensions={0}, use_global_device_ids=true | all-gather | bytes 655360 | tf_op jit(solution)/shard_map/all_gather | solution.py:25
  42.2 1.0 copy.17
  43.3 2.1 while.18
  43.3 2.0 conditional.3
  43.4 0.1 broadcast_compare_fusion
  43.6 0.7 fusion.13
  44.3 0.5 fusion.4
  44.9 0.4 fusion.3
  45.4 0.2 reshape.60
  45.6 0.2 copy.22
  45.7 7.2 %all_to_all.16 = bf16[4,64,256]{2,1,0:T(8,128)(2,1)S(1)} all-to-all(bf16[4,64,256]{2,1,0:T(8,128)(2,1)S(1)} %copy.22), channel_id=1, replica_groups=mesh['grp'=2,'sp'=4,'tp'=4] {'tp'}, dimensions={0} | all-to-all | bytes 262144 | tf_op jit(solution)/shard_map/all_to_all | solution.py:72
  52.9 3.2 multiply_reduce_fusion
  56.1 0.8 multiply_convert_fusion
  56.9 0.0 all-gather.5.cloned.1.call-update
  57.0 0.0 all-gather.7.cloned.1.call-start
  57.0 0.7 all-gather.7.cloned.1.call-update
  57.7 0.0 all-gather.11.cloned.1.call-start
  57.8 0.7 all-gather.11.cloned.1.call-update
  58.5 0.0 all-gather.9.cloned.1.call-start
  58.5 0.5 all-gather.9.cloned.1.call-update
  59.0 0.0 reduce-scatter.2.cloned.1.call-start
  59.1 16.3 %all-gather.5.cloned.1.call-done = bf16[256,2048]{1,0:T(8,128)(2,1)} async-done(((bf16[64,2048]{1,0:T(8,128)(2,1)}), bf16[256,2048]{1,0:T(8,128)(2,1)}) %all-gather.5.cloned.1.call-update) | async-done | bytes 1048592 | tf_op jit(solution)/shard_map/all_gather | solution.py:77
  75.3 108.3 %all-gather.7.cloned.1.call-done = bf16[2048,1408]{1,0:T(8,128)(2,1)} async-done(((bf16[512,1408]{1,0:T(8,128)(2,1)}), bf16[2048,1408]{1,0:T(8,128)(2,1)}) %all-gather.7.cloned.1.call-update) | async-done | bytes 5767184 | tf_op jit(solution)/shard_map/all_gather | solution.py:79
  183.6 4.8 %fusion.14 = f32[256,1408]{1,0:T(8,128)S(1)} fusion(bf16[256,2048]{1,0:T(8,128)(2,1)} %all-gather.5.cloned.1.call-done, bf16[2048,1408]{1,0:T(8,128)(2,1)} %all-gather.7.cloned.1.call-done), kind=kOutput, calls=%fused_computation.32 | convolution fusion | flops 1476395008 | bytes 8257536 | tf_op jit(solution)/shard_map/dot_general | solution.py:83
  188.4 101.8 %all-gather.11.cloned.1.call-done = bf16[1408,2048]{1,0:T(8,128)(2,1)} async-done(((bf16[1408,512]{1,0:T(8,128)(2,1)}), bf16[1408,2048]{1,0:T(8,128)(2,1)}) %all-gather.11.cloned.1.call-update) | async-done | bytes 5767184 | tf_op jit(solution)/shard_map/all_gather | solution.py:81
  290.2 106.4 %all-gather.9.cloned.1.call-done = bf16[2048,1408]{1,0:T(8,128)(2,1)} async-done(((bf16[512,1408]{1,0:T(8,128)(2,1)}), bf16[2048,1408]{1,0:T(8,128)(2,1)}) %all-gather.9.cloned.1.call-update) | async-done | bytes 5767184 | tf_op jit(solution)/shard_map/all_gather | solution.py:80
  396.6 8.8 %convolution_convert_fusion = bf16[256,2048]{1,0:T(8,128)(2,1)} fusion(bf16[1408,2048]{1,0:T(8,128)(2,1)} %all-gather.11.cloned.1.call-done, bf16[256,2048]{1,0:T(8,128)(2,1)S(1)} %copy-done.3, bf16[2048,1408]{1,0:T(8,128)(2,1)} %all-gather.9.cloned.1.call-done, f32[256,1408]{1,0:T(8,128)S(1)} %fusion.14), kind=kOutput, calls=%fused_computation.22 | convolution fusion | flops 2955476992 | bytes 15073280 | tf_op jit(solution)/shard_map/dot_general | solution.py:86
  405.4 23.2 %reduce-scatter.2.cloned.1.call-done = bf16[64,2048]{1,0:T(8,128)(2,1)} async-done(((bf16[256,2048]{1,0:T(8,128)(2,1)}), bf16[64,2048]{1,0:T(8,128)(2,1)}) %reduce-scatter.2.cloned.1.call-update) | async-done | bytes 262160 | tf_op jit(solution)/shard_map/reduce_scatter | solution.py:87
  428.6 1.7 add_convert_fusion
  (27 shorter events, 0.2 us)
Async XLA Ops:
  6.5 36.7 %copy-start.1 = (f32[1024,4]{0,1:T(4,128)S(1)}, f32[1024,4]{0,1:T(4,128)}, u32[]{:S(2)}) copy-start(f32[1024,4]{0,1:T(4,128)} %param.18) | copy-start | bytes 49156
  6.5 68.8 %all-gather.5.cloned.1.call-start = ((), (), s32[]{:S(2)}) async-start(), calls=%async_computation.2 | async-start | bytes 1310720 | tf_op jit(solution)/shard_map/all_gather | solution.py:77
  43.3 9.6 %copy-start = (bf16[64,2048]{1,0:T(8,128)(2,1)S(1)}, bf16[64,2048]{1,0:T(8,128)(2,1)}, u32[]{:S(2)}) copy-start(bf16[64,2048]{1,0:T(8,128)(2,1)} %param.14) | copy-start | bytes 786436
  52.9 3.2 copy-start.2
  57.0 126.7 %all-gather.7.cloned.1.call-start = ((), (), s32[]{:S(2)}) async-start(), calls=%async_computation.3 | async-start | bytes 7208960 | tf_op jit(solution)/shard_map/all_gather | solution.py:79
  57.7 232.5 %all-gather.11.cloned.1.call-start = ((), (), s32[]{:S(2)}) async-start(), calls=%async_computation.5 | async-start | bytes 7208960 | tf_op jit(solution)/shard_map/all_gather | solution.py:81
  58.5 338.1 %all-gather.9.cloned.1.call-start = ((), (), s32[]{:S(2)}) async-start(), calls=%async_computation.4 | async-start | bytes 7208960 | tf_op jit(solution)/shard_map/all_gather | solution.py:80
  59.0 369.6 %reduce-scatter.2.cloned.1.call-start = ((), (), s32[]{:S(2)}) async-start(), calls=%async_computation.6 | async-start | bytes 1310720 | tf_op jit(solution)/shard_map/reduce_scatter | solution.py:87
  75.3 321.2 %copy-start.3 = (bf16[256,2048]{1,0:T(8,128)(2,1)S(1)}, bf16[256,2048]{1,0:T(8,128)(2,1)}, u32[]{:S(2)}) copy-start(bf16[256,2048]{1,0:T(8,128)(2,1)} %all-gather.5.cloned.1.call-done) | copy-start | bytes 3145732
Sparse Core Ops, SparseCore 0:
  57.1 18.2 all-gather.4
  76.9 106.6 all-gather.6
  185.2 104.9 all-gather.10
  291.6 104.9 all-gather.8
  405.5 23.0 reduce-scatter.1
where the time goes:
time: 437 us
  waiting for transfers between devices  358 us (82%)
  blocking collectives  40.8 us (9%)
  matrix products  18 us (4%)
  between operations  13.3 us (3%)
    all_gather x1, waiting for transfers between devices, on_device(): lax.all_gather(w_gate, 'sp', axis=0, tiled=True)  108 us
    all_gather x1, waiting for transfers between devices, on_device(): lax.all_gather(w_up, 'sp', axis=0, tiled=True)  106 us
    all_gather x1, waiting for transfers between devices, on_device(): lax.all_gather(w_down, 'sp', axis=1, tiled=True)  102 us
    reduce_scatter x1, waiting for transfers between devices, on_device(): lax.psum_scatter(terms.astype(jnp.bfloat16), 'tp', scatter_dimension=0, t...  23.2 us
    all_gather x1, blocking collectives, on_device(): key_piece = lax.all_gather(keys, 'sp', axis=0, tiled=True)  17.4 us
    all_gather x1, waiting for transfers between devices, on_device(): all_rows = lax.all_gather(normed, 'tp', axis=0, tiled=True)  16.3 us
    all_gather x1, blocking collectives, on_device(): value_piece = lax.all_gather(values, 'sp', axis=0, tiled=True)  16.3 us
    dot_general x1, matrix products, on_device(): terms = jnp.dot(hidden, full_down, preferred_element_type=jnp.float32)  8.81 us
  transfers between devices with their start and end apart: 5, of which 5 were waited for; matrix products, arithmetic and copies ran while one was open for 1% of the time, Pallas kernels for 0%

commit v1 on v0

--- a/solution.py
+++ b/solution.py
@@ -78,7 +78,7 @@
     full_gate, full_up, full_down = (
         lax.all_gather(w_gate, "sp", axis=0, tiled=True),
         lax.all_gather(w_up, "sp", axis=0, tiled=True),
-        lax.all_gather(w_down, "sp", axis=1, tiled=True),
+        jnp.concatenate(lax.all_gather(w_down, "sp"), axis=1),
     )
     gate = jnp.dot(all_rows, full_gate, preferred_element_type=jnp.float32)
     up = jnp.dot(all_rows, full_up, preferred_element_type=jnp.float32)

time: 437 us -> 402 us (0.920)
  waiting for transfers between devices: 358 us -> 302 us
  blocking collectives: 40.8 us -> 52.5 us
  local copies, waits for them, and re-layouts: 3.45 us -> 11.8 us
    all_gather x1, waiting for transfers between devices: 102 us -> 58.1 us  [on_device(): lax.all_gather(w_down, 'sp')]
    reshape x0 -> x1, local copies, waits for them, and re-layouts: none -> 8.32 us  [on_device(): jnp.concatenate(lax.all_gather(w_down, 'sp'), axis=1)]
    all_gather x1, blocking collectives: 16.3 us -> 24.2 us  [on_device(): value_piece = lax.all_gather(values, 'sp', axis=0, tiled=True)]
    all_gather x1, waiting for transfers between devices: 16.3 us -> 9.05 us  [on_device(): all_rows = lax.all_gather(normed, 'tp', axis=0, tiled=True)]
    all_gather x1, waiting for transfers between devices: 106 us -> 102 us  [on_device(): lax.all_gather(w_up, 'sp', axis=0, tiled=True)]
  transfers between devices with their start and end apart: 5 -> 5, of which waited for: 5 -> 5; matrix products, arithmetic and copies ran while one was open for 1% -> 6% of each run, Pallas kernels for 0% -> 0%
where the time goes in v1:
time: 402 us; the launch traced here: 401 us
  waiting for transfers between devices  302 us (75%)
  blocking collectives  52.5 us (13%)
  matrix products  18 us (4%)
  between operations  13.3 us (3%)
  local copies, waits for them, and re-layouts  11.8 us (3%)
    all_gather x1, waiting for transfers between devices, on_device(): lax.all_gather(w_gate, 'sp', axis=0, tiled=True)  108 us
    all_gather x1, waiting for transfers between devices, on_device(): lax.all_gather(w_up, 'sp', axis=0, tiled=True)  102 us
    all_gather x1, waiting for transfers between devices, on_device(): lax.all_gather(w_down, 'sp')  58.1 us
    all_gather x1, blocking collectives, on_device(): value_piece = lax.all_gather(values, 'sp', axis=0, tiled=True)  24.2 us
    reduce_scatter x1, waiting for transfers between devices, on_device(): lax.psum_scatter(terms.astype(jnp.bfloat16), 'tp', scatter_dimension=0, t...  23.2 us
    all_gather x1, blocking collectives, on_device(): key_piece = lax.all_gather(keys, 'sp', axis=0, tiled=True)  21.3 us
    all_gather x1, waiting for transfers between devices, on_device(): all_rows = lax.all_gather(normed, 'tp', axis=0, tiled=True)  9.05 us
    dot_general x1, matrix products, on_device(): terms = jnp.dot(hidden, full_down, preferred_element_type=jnp.float32)  8.77 us
  transfers between devices with their start and end apart: 5, of which 5 were waited for; matrix products, arithmetic and copies ran while one was open for 6% of the time, Pallas kernels for 0%

profile of v1, /device:TPU:0, one launch (start us, length us, event | category | flops | bytes accessed | tf_op | source)
XLA Modules:
  0.0 401.2 jit_solution(9746494457292121686)
XLA Ops:
  6.5 0.7 all-gather.12.cloned.1.call-update
  7.3 0.0 all-gather.6.cloned.1.call-start
  7.3 1.0 copy.22
  8.3 1.0 copy.24
  9.3 1.0 copy.23
  10.4 21.3 %all_gather.21 = bf16[1024,256]{0,1:T(8,128)(2,1)S(1)} all-gather(bf16[256,256]{0,1:T(8,128)(2,1)S(1)} %copy.22), channel_id=1, replica_groups=mesh['grp'=2,'sp'=4,'tp'=4] {'sp'}, dimensions={0}, use_global_device_ids=true | all-gather | bytes 655360 | tf_op jit(solution)/shard_map/all_gather | solution.py:24
  31.7 24.2 %all_gather.22 = bf16[1024,256]{0,1:T(8,128)(2,1)S(1)} all-gather(bf16[256,256]{0,1:T(8,128)(2,1)S(1)} %copy.24), channel_id=1, replica_groups=mesh['grp'=2,'sp'=4,'tp'=4] {'sp'}, dimensions={0}, use_global_device_ids=true | all-gather | bytes 655360 | tf_op jit(solution)/shard_map/all_gather | solution.py:25
  55.9 2.1 while.18
  56.0 2.0 conditional.3
  56.1 0.1 broadcast_compare_fusion
  56.2 0.7 fusion.13
  57.0 0.5 fusion.4
  57.5 0.4 fusion.3
  58.0 0.2 reshape.69
  58.2 0.2 copy.29
  58.4 7.0 %all_to_all.16 = bf16[4,64,256]{2,1,0:T(8,128)(2,1)S(1)} all-to-all(bf16[4,64,256]{2,1,0:T(8,128)(2,1)S(1)} %copy.29), channel_id=1, replica_groups=mesh['grp'=2,'sp'=4,'tp'=4] {'tp'}, dimensions={0} | all-to-all | bytes 262144 | tf_op jit(solution)/shard_map/all_to_all | solution.py:72
  65.4 3.2 multiply_reduce_fusion
  68.6 0.8 multiply_convert_fusion
  69.4 0.0 all-gather.8.cloned.1.call-start
  69.5 0.7 all-gather.8.cloned.1.call-update
  70.2 0.0 all-gather.10.cloned.1.call-start
  70.2 0.5 all-gather.10.cloned.1.call-update
  70.7 0.0 reduce-scatter.2.cloned.1.call-start
  70.8 58.1 %all-gather.12.cloned.1.call-done = bf16[5632,512]{1,0:T(8,128)(2,1)} async-done(((bf16[1408,512]{1,0:T(8,128)(2,1)}), bf16[5632,512]{1,0:T(8,128)(2,1)}) %all-gather.12.cloned.1.call-update) | async-done | bytes 5767184 | tf_op jit(solution)/shard_map/all_gather | solution.py:81
  128.9 8.3 %copy.27 = bf16[1408,4,512]{0,2,1:T(8,128)(2,1)} copy(bf16[1408,4,512]{2,0,1:T(8,128)(2,1)} %bitcast.37) | data formatting | bytes 11534336 | tf_op jit(solution)/shard_map/reshape | solution.py:81
  137.2 9.0 %all-gather.6.cloned.1.call-done = bf16[256,2048]{1,0:T(8,128)(2,1)} async-done(((bf16[64,2048]{1,0:T(8,128)(2,1)}), bf16[256,2048]{1,0:T(8,128)(2,1)}) %all-gather.6.cloned.1.call-update) | async-done | bytes 1048592 | tf_op jit(solution)/shard_map/all_gather | solution.py:77
  146.3 108.3 %all-gather.8.cloned.1.call-done = bf16[2048,1408]{1,0:T(8,128)(2,1)} async-done(((bf16[512,1408]{1,0:T(8,128)(2,1)}), bf16[2048,1408]{1,0:T(8,128)(2,1)}) %all-gather.8.cloned.1.call-update) | async-done | bytes 5767184 | tf_op jit(solution)/shard_map/all_gather | solution.py:79
  254.6 4.8 %fusion.14 = f32[256,1408]{1,0:T(8,128)S(1)} fusion(bf16[256,2048]{1,0:T(8,128)(2,1)} %all-gather.6.cloned.1.call-done, bf16[2048,1408]{1,0:T(8,128)(2,1)} %all-gather.8.cloned.1.call-done), kind=kOutput, calls=%fused_computation.32 | convolution fusion | flops 1476395008 | bytes 8257536 | tf_op jit(solution)/shard_map/dot_general | solution.py:83
  259.4 101.6 %all-gather.10.cloned.1.call-done = bf16[2048,1408]{1,0:T(8,128)(2,1)} async-done(((bf16[512,1408]{1,0:T(8,128)(2,1)}), bf16[2048,1408]{1,0:T(8,128)(2,1)}) %all-gather.10.cloned.1.call-update) | async-done | bytes 5767184 | tf_op jit(solution)/shard_map/all_gather | solution.py:80
  361.0 8.8 %convolution_convert_fusion = bf16[256,2048]{1,0:T(8,128)(2,1)} fusion(bf16[1408,2048]{0,1:T(8,128)(2,1)} %bitcast.38, bf16[256,2048]{1,0:T(8,128)(2,1)S(1)} %copy-done.3, bf16[2048,1408]{1,0:T(8,128)(2,1)} %all-gather.10.cloned.1.call-done, f32[256,1408]{1,0:T(8,128)S(1)} %fusion.14), kind=kOutput, calls=%fused_computation.22 | convolution fusion | flops 2955476992 | bytes 15073280 | tf_op jit(solution)/shard_map/dot_general | solution.py:86
  369.8 23.2 %reduce-scatter.2.cloned.1.call-done = bf16[64,2048]{1,0:T(8,128)(2,1)} async-done(((bf16[256,2048]{1,0:T(8,128)(2,1)}), bf16[64,2048]{1,0:T(8,128)(2,1)}) %reduce-scatter.2.cloned.1.call-update) | async-done | bytes 262160 | tf_op jit(solution)/shard_map/reduce_scatter | solution.py:87
  393.0 1.7 add_convert_fusion
  (28 shorter events, 0.2 us)
Async XLA Ops:
  6.5 3.8 copy-start.1
  6.5 122.4 %all-gather.12.cloned.1.call-start = ((), (), s32[]{:S(2)}) async-start(), calls=%async_computation.6 | async-start | bytes 7208960 | tf_op jit(solution)/shard_map/all_gather | solution.py:81
  7.3 139.0 %all-gather.6.cloned.1.call-start = ((), (), s32[]{:S(2)}) async-start(), calls=%async_computation.2 | async-start | bytes 1310720 | tf_op jit(solution)/shard_map/all_gather | solution.py:77
  55.9 9.5 %copy-start = (bf16[64,2048]{1,0:T(8,128)(2,1)S(1)}, bf16[64,2048]{1,0:T(8,128)(2,1)}, u32[]{:S(2)}) copy-start(bf16[64,2048]{1,0:T(8,128)(2,1)} %param.14) | copy-start | bytes 786436
  65.4 3.2 copy-start.2
  69.4 185.2 %all-gather.8.cloned.1.call-start = ((), (), s32[]{:S(2)}) async-start(), calls=%async_computation.3 | async-start | bytes 7208960 | tf_op jit(solution)/shard_map/all_gather | solution.py:79
  70.2 290.8 %all-gather.10.cloned.1.call-start = ((), (), s32[]{:S(2)}) async-start(), calls=%async_computation.4 | async-start | bytes 7208960 | tf_op jit(solution)/shard_map/all_gather | solution.py:80
  70.7 322.2 %reduce-scatter.2.cloned.1.call-start = ((), (), s32[]{:S(2)}) async-start(), calls=%async_computation.5 | async-start | bytes 1310720 | tf_op jit(solution)/shard_map/reduce_scatter | solution.py:87
  146.3 214.7 %copy-start.3 = (bf16[256,2048]{1,0:T(8,128)(2,1)S(1)}, bf16[256,2048]{1,0:T(8,128)(2,1)}, u32[]{:S(2)}) copy-start(bf16[256,2048]{1,0:T(8,128)(2,1)} %all-gather.6.cloned.1.call-done) | copy-start | bytes 3145732
Sparse Core Ops, SparseCore 0:
  8.9 119.9 all-gather.11
  130.5 15.7 all-gather.5
  147.9 106.6 all-gather.7
  256.0 104.9 all-gather.9
  369.9 23.0 reduce-scatter.1
